TPU v7x, 256 devices: a whole 4x4x8 slice. The times are simulated.
256 devices in a mesh: ep: 64 (over z, y, core), tp: 4 (over x).
Axes of the slice: x: 4, y: 4, z: 8, core: 2. Of those that a mesh axis runs over, the one named last changes fastest.
Arguments:
- mixer_input: bfloat16 [32768, 2048], P('ep'), may hold values from -6 to 6
- mixer_gain: bfloat16 [2048], replicated, may hold values from 0.099609375 to 1.8984375
- pool_in: bfloat16 [2048, 1024], P(None, 'tp'), may hold values from -0.125 to 0.125
- pool_map: bfloat16 [4, 256, 256], P('tp'), may hold values from -0.375 to 0.375
- pool_scale: bfloat16 [1024], P('tp'), may hold values from 0.099609375 to 1.8984375
- pool_out: bfloat16 [1024, 2048], P('tp'), may hold values from -0.1875 to 0.1875
- expert_input: bfloat16 [24576, 2048], P('ep'), may hold values from -6 to 6
- expert_gain: bfloat16 [2048], replicated, may hold values from 0.099609375 to 1.8984375
- group_router: bfloat16 [2048, 4], replicated, may hold values from -0.125 to 0.125
- expert_router: bfloat16 [2048, 64], replicated, may hold values from -0.125 to 0.125
- routes: int32 [24576, 2], P('ep'), may hold values from 0 to 63, all different within a row; in each aligned block of 96 rows (0 to 95, 96 to 191, ...) at most 6 rows name the same one
- gate_weight: bfloat16 [64, 2048, 1024], P('ep', None, 'tp'), may hold values from -0.125 to 0.125
- up_weight: bfloat16 [64, 2048, 1024], P('ep', None, 'tp'), may hold values from -0.125 to 0.125
- down_weight: bfloat16 [64, 1024, 2048], P('ep', 'tp'), may hold values from -0.1875 to 0.1875
Outputs:
- mixer_output: bfloat16 [32768, 2048], P(('ep', 'tp'))
- expert_output: bfloat16 [24576, 2048], P(('ep', 'tp'))
Inputs may be any that keep to these rules, and one draw needn't show every extreme that they name: `routes`: each row names two different experts. In each aligned block of 96 rows no expert is named more than 6 times, a bound that some block reaches.
All inputs are finite; a program needn't handle non-finite values.
Results may differ from a plain program's by a relative error of at most 0.01.
Values may be sent and summed in bfloat16 or wider, within the bound.
No kernel may reach another device: no remote copies, remote signals or barrier semaphores. Data moves between devices by JAX's collectives and lax.ppermute only.
A program may use at most 64 MiB of HBM per device.

v0:
```python
import jax
import jax.numpy as jnp
from jax import lax
from jax.sharding import PartitionSpec as P

RIM = 15
EPS = 1e-06


def passed_along(value, axis, steps):
    count = lax.axis_size(axis)
    leading, last = (max(0, -steps), min(count, count - steps))
    return lax.ppermute(value, axis, [(source, source + steps) for source in range(leading, last)])


def norm_rows(values, gain):
    floats = values.astype(jnp.float32)
    scale = lax.rsqrt(jnp.mean(floats * floats, axis=-1, keepdims=True) + EPS)
    return (floats * scale * gain.astype(jnp.float32)).astype(jnp.bfloat16)


def route_weights(rows, group_router, expert_router, route_rows):
    group_logits = jnp.dot(rows, group_router, preferred_element_type=jnp.float32)
    expert_logits = jnp.dot(rows, expert_router, preferred_element_type=jnp.float32)
    groups = group_logits.shape[1]
    experts = expert_logits.shape[1]
    member = (
        jnp.arange(experts, dtype=jnp.int32)[:, None] // (experts // groups)
        == jnp.arange(groups, dtype=jnp.int32)[None, :]
    ).astype(jnp.float32)
    group_exp = jnp.exp(group_logits)
    group_prob = group_exp / jnp.sum(group_exp, axis=1, keepdims=True)
    expert_exp = jnp.exp(expert_logits)
    within = jnp.dot(expert_exp, member, precision=lax.Precision.HIGHEST)
    prob = expert_exp * jnp.dot(group_prob / within, member.T, precision=lax.Precision.HIGHEST)
    chosen = (route_rows[:, :, None] == jnp.arange(experts, dtype=jnp.int32)[None, None, :]).astype(
        jnp.float32
    )
    picked = jnp.sum(chosen * prob[:, None, :], axis=2)
    return picked / jnp.sum(picked, axis=1, keepdims=True)


def mixer_half(mixer_input, mixer_gain, pool_in, pool_map, pool_scale, pool_out):
    normed = norm_rows(mixer_input, mixer_gain)
    pooled_in = jnp.dot(normed, pool_in, preferred_element_type=jnp.float32).astype(jnp.bfloat16)
    local_rows = pooled_in.shape[0]
    groups_here = pool_map.shape[0]
    channels = pool_map.shape[1]
    border = passed_along(pooled_in[local_rows - RIM :], "ep", 1)
    padded = jnp.concatenate([border, pooled_in], axis=0).astype(jnp.float32)
    padded = padded.reshape(local_rows + RIM, groups_here, channels)
    leading = lax.axis_index("tp") * groups_here
    windows = jnp.left_shift(jnp.int32(2), leading + jnp.arange(groups_here, dtype=jnp.int32))
    window_sum = jnp.zeros((local_rows, groups_here, channels), jnp.float32)
    for offset in range(RIM + 1):
        active = (offset < windows).astype(jnp.float32)
        window_sum = (
            window_sum + padded[RIM - offset : RIM - offset + local_rows] * active[None, :, None]
        )
    position = lax.axis_index("ep") * local_rows + jnp.arange(local_rows, dtype=jnp.int32)
    counts_here = jnp.minimum(position[:, None] + 1, windows[None, :]).astype(jnp.float32)
    pooled = (window_sum / counts_here[:, :, None] - padded[RIM:]).astype(jnp.bfloat16)
    mapped = jnp.einsum("tgc,gce->tge", pooled, pool_map, preferred_element_type=jnp.float32)
    mixed_rows = (
        mapped.reshape(local_rows, groups_here * channels) * pool_scale.astype(jnp.float32)
    ).astype(jnp.bfloat16)
    return lax.psum_scatter(
        jnp.dot(mixed_rows, pool_out, preferred_element_type=jnp.float32).astype(jnp.bfloat16),
        "tp",
        scatter_dimension=0,
        tiled=True,
    )


def slot_positions(route_rows, blocks, experts):
    flat = route_rows.reshape(blocks, -1)
    onehot = (flat[:, :, None] == jnp.arange(experts, dtype=jnp.int32)[None, None, :]).astype(
        jnp.int32
    )
    before = jnp.cumsum(onehot, axis=1) - onehot
    return (jnp.sum(before * onehot, axis=2), flat)


def dispatch_rows(normed, route_rows, blocks, slots_each, experts):
    block_len = normed.shape[0] // blocks
    positions, flat = slot_positions(route_rows, blocks, experts)
    block_index = jnp.arange(blocks, dtype=jnp.int32)[:, None]
    slot_index = block_index * slots_each + positions
    token_index = block_index * block_len + jnp.arange(2 * block_len, dtype=jnp.int32)[None, :] // 2
    table = jnp.full((blocks * slots_each, experts), -1, jnp.int32)
    table = table.at[slot_index.reshape(-1), flat.reshape(-1)].set(token_index.reshape(-1))
    fetched = normed[jnp.maximum(table, 0)]
    return jnp.where((table >= 0)[:, :, None], fetched, jnp.zeros_like(fetched))


def expert_half(
    expert_input,
    expert_gain,
    group_router,
    expert_router,
    routes,
    gate_weight,
    up_weight,
    down_weight,
):
    normed = norm_rows(expert_input, expert_gain)
    tp_count = lax.axis_size("tp")
    tp_place = lax.axis_index("tp")
    experts = expert_router.shape[1]
    block_len = normed.shape[0] // tp_count
    slots_each = 4 * block_len // experts
    own_rows = lax.dynamic_slice_in_dim(normed, tp_place * block_len, block_len, 0)
    own_routes = lax.dynamic_slice_in_dim(routes, tp_place * block_len, block_len, 0)
    sending = dispatch_rows(own_rows, own_routes, 1, slots_each, experts)
    arrived = lax.all_to_all(sending, "ep", split_axis=1, concat_axis=1, tiled=True)
    received = lax.all_gather(arrived, "tp", axis=0, tiled=True)
    held = gate_weight.shape[0]
    model = received.shape[2]
    down_whole = lax.all_gather(down_weight, "tp", axis=1, tiled=True)
    all_slots = received.reshape(received.shape[0], -1, held, model)
    gate = jnp.einsum("csed,edh->cseh", all_slots, gate_weight, preferred_element_type=jnp.float32)
    upward = jnp.einsum("csed,edh->cseh", all_slots, up_weight, preferred_element_type=jnp.float32)
    hidden = (jax.nn.silu(gate) * upward).astype(jnp.bfloat16)
    swapped = lax.all_to_all(hidden, "tp", split_axis=0, concat_axis=3, tiled=True)
    hid_part = hidden.shape[3]
    total = jnp.zeros((swapped.shape[0], swapped.shape[1], held, model), jnp.float32)
    for part in range(tp_count):
        partial_value = jnp.einsum(
            "cseh,ehd->csed",
            swapped[:, :, :, part * hid_part : (part + 1) * hid_part],
            down_whole[:, part * hid_part : (part + 1) * hid_part],
            preferred_element_type=jnp.float32,
        ).astype(jnp.bfloat16)
        partial_value = lax.optimization_barrier(partial_value)
        total = total + partial_value.astype(jnp.float32)
    summed = total.astype(jnp.bfloat16).reshape(slots_each, -1, model)
    returned = lax.all_to_all(summed, "ep", split_axis=1, concat_axis=1, tiled=True)
    positions, flat = slot_positions(own_routes, 1, experts)
    lookup = positions[0] * experts + flat[0]
    picked = (
        returned.reshape(slots_each * experts, model)[lookup]
        .astype(jnp.float32)
        .reshape(block_len, 2, model)
    )
    weights = route_weights(own_rows, group_router, expert_router, own_routes)
    return jnp.sum(picked * weights[:, :, None], axis=1).astype(jnp.bfloat16)


def on_device(
    mixer_input,
    mixer_gain,
    pool_in,
    pool_map,
    pool_scale,
    pool_out,
    expert_input,
    expert_gain,
    group_router,
    expert_router,
    routes,
    gate_weight,
    up_weight,
    down_weight,
):
    mixer_output = mixer_half(mixer_input, mixer_gain, pool_in, pool_map, pool_scale, pool_out)
    expert_output = expert_half(
        expert_input,
        expert_gain,
        group_router,
        expert_router,
        routes,
        gate_weight,
        up_weight,
        down_weight,
    )
    return (mixer_output, expert_output)


def solution(mesh):
    return jax.shard_map(
        on_device,
        mesh=mesh,
        in_specs=(
            P("ep", None),
            P(),
            P(None, "tp"),
            P("tp", None, None),
            P("tp"),
            P("tp", None),
            P("ep", None),
            P(),
            P(),
            P(),
            P("ep", None),
            P("ep", None, "tp"),
            P("ep", None, "tp"),
            P("ep", "tp", None),
        ),
        out_specs=(P(("ep", "tp"), None), P(("ep", "tp"), None)),
        check_vma=False,
    )
```

profile of v0, /device:TPU:8, one launch (start us, length us, event | category | flops | bytes accessed | tf_op | source)
XLA Modules:
  0.0 302.8 jit_solution(5306408200580199578)
XLA Ops:
  7.2 0.9 constant_dynamic-slice_fusion
  9.5 1.8 multiply_reduce_fusion
  11.3 2.0 convert_element_type.227
  13.9 9.3 %scatter_fusion = s32[6,64]{1,0:T(8,128)S(1)} fusion(s32[6,64]{1,0:T(8,128)S(1)} %broadcast_in_dim.11, s32[192]{0:T(256)S(1)} %bitcast.129, s32[192]{0:T(256)S(1)} %and_select_fusion.1), kind=kCustom, calls=%fused_computation.2 | custom fusion | bytes 3840 | tf_op jit(solution)/shard_map/scatter | solution.py:91
  23.5 1.3 fusion.26
  24.8 2.5 gather_fusion
  27.2 1.0 copy_select_fusion
  28.2 63.1 %all_to_all.28 = bf16[6,64,2048]{2,0,1:T(8,128)(2,1)S(1)} all-to-all(bf16[6,64,2048]{2,0,1:T(8,128)(2,1)S(1)} %copy_select_fusion), channel_id=1, replica_groups=mesh['ep'=64,'tp'=4] {'ep'}, dimensions={1} | all-to-all | bytes 3145728 | tf_op jit(solution)/shard_map/all_to_all | solution.py:115
  91.4 2.0 copy.48
  93.5 0.7 all-gather.5.cloned.1.call-update
  94.2 0.8 copy-done.3
  95.6 0.8 fusion.17
  96.4 0.7 copy-done.4
  97.1 1.9 collective-permute-start
  99.1 58.8 %all-gather.3.cloned.1.call-done = bf16[24,64,2048]{2,1,0:T(8,128)(2,1)} async-done(((bf16[6,64,2048]{2,1,0:T(8,128)(2,1)}), bf16[24,64,2048]{2,1,0:T(8,128)(2,1)}) %all-gather.3.cloned.1.call-update) | async-done | bytes 6291472 | tf_op jit(solution)/shard_map/all_gather | solution.py:116
  157.9 5.1 %fusion.23 = f32[24,64,256]{2,1,0:T(8,128)S(1)} fusion(bf16[24,64,2048]{2,1,0:T(8,128)(2,1)} %all-gather.3.cloned.1.call-done, bf16[1,2048,256]{2,1,0:T(8,128)(2,1)} %param.25), kind=kOutput, calls=%fused_computation.46 | convolution fusion | flops 1610612736 | bytes 8912896 | tf_op jit(solution)/shard_map/csed,edh->cseh/dot_general | solution.py:121
  163.1 3.0 fusion.16
  166.1 3.8 %all-to-all-start.1 = ((bf16[24,64,1,256]{3,1,2,0:T(8,128)(2,1)}), bf16[24,64,1,256]{3,1,2,0:T(8,128)(2,1)S(1)}, u32[]{:S(2)}, u32[]{:S(2)}) async-start(bf16[24,64,1,256]{3,1,2,0:T(8,128)(2,1)} %fusion.16), calls=%async_computation.2 | async-start | bytes 1572864 | tf_op jit(solution)/shard_map/all_to_all | solution.py:124
  170.0 3.3 %convolution_convert_fusion = bf16[512,2048]{1,0:T(8,128)(2,1)} fusion(bf16[256,2048]{1,0:T(8,128)(2,1)S(1)} %copy-done, f32[256]{0:T(256)S(1)} %convert_element_type.223, f32[527,256]{1,0:T(8,128)S(1)} %maximum_convert_fusion, f32[512]{0:T(512)S(1)} %minimum_convert_fusion, f32[]{:T(128)S(6)} %convert_element_type.220, f32[]{:T(128)S(6)} %convert_element_type.219, ...), kind=kOutput, calls=%fused_computation.10 | convolution fusion | flops 609746944 | bytes 11668544 | tf_op jit(solution)/shard_map/dot_general | solution.py:68
  173.4 14.8 %all-to-all-done.1 = bf16[24,64,1,256]{3,1,2,0:T(8,128)(2,1)S(1)} async-done(((bf16[24,64,1,256]{3,1,2,0:T(8,128)(2,1)}), bf16[24,64,1,256]{3,1,2,0:T(8,128)(2,1)S(1)}, u32[]{:S(2)}, u32[]{:S(2)}) %all-to-all-start.1) | async-done | bytes 786464 | tf_op jit(solution)/shard_map/all_to_all | solution.py:124
  188.2 0.6 copy.56
  189.4 26.5 %all-gather.5.cloned.1.call-done = bf16[1,1024,2048]{2,1,0:T(8,128)(2,1)} async-done(((bf16[1,256,2048]{2,1,0:T(8,128)(2,1)}), bf16[1,1024,2048]{2,1,0:T(8,128)(2,1)}) %all-gather.5.cloned.1.call-update) | async-done | bytes 4194320 | tf_op jit(solution)/shard_map/all_gather | solution.py:119
  215.8 2.0 fusion.3
  217.8 1.8 fusion.4
  220.8 1.4 fusion.11
  222.2 2.2 copy.51
  224.4 10.9 %all-to-all-start.2 = ((bf16[6,64,2048]{2,0,1:T(8,128)(2,1)}), bf16[6,64,2048]{2,0,1:T(8,128)(2,1)}, u32[]{:S(2)}, u32[]{:S(2)}) async-start(bf16[6,64,2048]{2,0,1:T(8,128)(2,1)} %copy.51), calls=%async_computation.3 | async-start | bytes 4194304 | tf_op jit(solution)/shard_map/all_to_all | solution.py:137
  236.5 49.9 %all-to-all-done.2 = bf16[6,64,2048]{2,0,1:T(8,128)(2,1)} async-done(((bf16[6,64,2048]{2,0,1:T(8,128)(2,1)}), bf16[6,64,2048]{2,0,1:T(8,128)(2,1)}, u32[]{:S(2)}, u32[]{:S(2)}) %all-to-all-start.2) | async-done | bytes 1572896 | tf_op jit(solution)/shard_map/all_to_all | solution.py:137
  286.4 2.5 copy.52
  288.9 2.1 gather_fusion.1
  290.9 2.1 reshape.556
  293.1 3.1 %multiply_reduce_fusion.1 = bf16[96,2048]{1,0:T(8,128)(2,1)} fusion(f32[96,2,2048]{2,1,0:T(2,128)S(1)} %reshape.556, f32[96,2]{1,0:T(8,128)S(1)} %copy.53), kind=kLoop, calls=%fused_computation.31 | loop fusion | flops 589824 | bytes 1966848 | tf_op jit(solution)/shard_map/reduce_sum | solution.py:146
  (80 shorter events, 6.0 us)
Async XLA Ops:
  7.2 162.9 %copy-start = (bf16[256,2048]{1,0:T(8,128)(2,1)S(1)}, bf16[256,2048]{1,0:T(8,128)(2,1)}, u32[]{:S(2)}) copy-start(bf16[256,2048]{1,0:T(8,128)(2,1)} %param.19) | copy-start | bytes 3145732
  7.2 4.2 %copy-start.1 = (bf16[384,2048]{1,0:T(8,128)(2,1)S(1)}, bf16[384,2048]{1,0:T(8,128)(2,1)}, u32[]{:S(2)}) copy-start(bf16[384,2048]{1,0:T(8,128)(2,1)} %param.20) | copy-start | bytes 4718596
  7.2 150.7 %all-gather.3.cloned.1.call-start = ((), (), s32[]{:S(2)}) async-start(), calls=%async_computation.5 | async-start | bytes 7864320 | tf_op jit(solution)/shard_map/all_gather | solution.py:116
  13.4 10.0 %copy-start.8 = (bf16[2048]{0:T(1024)(128)(2,1)S(1)}, bf16[2048]{0:T(1024)(128)(2,1)}, u32[]{:S(2)}) copy-start(bf16[2048]{0:T(1024)(128)(2,1)} %param.21) | copy-start | bytes 12292
  93.4 0.8 copy-start.9
  93.4 1.6 copy-start.3
  93.4 122.4 %all-gather.5.cloned.1.call-start = ((), (), s32[]{:S(2)}) async-start(), calls=%async_computation.6 | async-start | bytes 5242880 | tf_op jit(solution)/shard_map/all_gather | solution.py:119
  94.2 1.4 copy-start.11
  95.6 3.5 %copy-start.14 = (bf16[256]{0:T(256)(128)(2,1)S(1)}, bf16[256]{0:T(256)(128)(2,1)}, u32[]{:S(2)}) copy-start(bf16[256]{0:T(256)(128)(2,1)} %param.18) | copy-start | bytes 1540
  96.4 0.7 copy-start.4
  97.1 72.9 %collective-permute-start = (bf16[15,256]{1,0:T(8,128)(2,1)S(1)}, bf16[15,256]{1,0:T(8,128)(2,1)S(1)}, u32[]{:S(2)}, u32[]{:S(2)}) collective-permute-start(bf16[15,256]{1,0:T(8,128)(2,1)S(1)} %slice.135), channel_id=1, source_target_pairs={{0,4},{4,8},{8,12},{12,16},{16,20},{20,24},{24,28},{28,32},{32,36}... | collective-permute-start | bytes 23048 | tf_op jit(solution)/shard_map/ppermute | solution.py:13
  157.9 5.1 %copy-start.10 = (bf16[24,64,2048]{2,1,0:T(8,128)(2,1)S(1)}, bf16[24,64,2048]{2,1,0:T(8,128)(2,1)}, u32[]{:S(2)}) copy-start(bf16[24,64,2048]{2,1,0:T(8,128)(2,1)} %all-gather.3.cloned.1.call-done) | copy-start | bytes 18874372
  157.9 5.1 %copy-start.12 = (bf16[1,2048,256]{2,1,0:T(8,128)(2,1)S(1)}, bf16[1,2048,256]{2,1,0:T(8,128)(2,1)}, u32[]{:S(2)}) copy-start(bf16[1,2048,256]{2,1,0:T(8,128)(2,1)} %param.26) | copy-start | bytes 3145732
  163.1 6.9 %copy-start.5 = (bf16[512,256]{1,0:T(8,128)(2,1)S(1)}, bf16[512,256]{1,0:T(8,128)(2,1)}, u32[]{:S(2)}) copy-start(bf16[512,256]{1,0:T(8,128)(2,1)} %copy-done.4) | copy-start | bytes 786436
  166.1 4.0 %copy-start.13 = (bf16[1,256,256]{2,1,0:T(8,128)(2,1)S(1)}, bf16[1,256,256]{2,1,0:T(8,128)(2,1)}, u32[]{:S(2)}) copy-start(bf16[1,256,256]{2,1,0:T(8,128)(2,1)} %param.17) | copy-start | bytes 393220
  166.1 22.1 %all-to-all-start.1 = ((bf16[24,64,1,256]{3,1,2,0:T(8,128)(2,1)}), bf16[24,64,1,256]{3,1,2,0:T(8,128)(2,1)S(1)}, u32[]{:S(2)}, u32[]{:S(2)}) async-start(bf16[24,64,1,256]{3,1,2,0:T(8,128)(2,1)} %fusion.16), calls=%async_computation.2 | async-start | bytes 1572864 | tf_op jit(solution)/shard_map/all_to_all | solution.py:124
  169.9 126.4 %reduce-scatter.2.cloned.1.call-start = ((), (), s32[]{:S(2)}) async-start(), calls=%async_computation.4 | async-start | bytes 2621440 | tf_op jit(solution)/shard_map/reduce_scatter | solution.py:67
  215.8 3.8 %copy-start.2 = (bf16[1,1024,2048]{2,1,0:T(8,128)(2,1)S(1)}, bf16[1,1024,2048]{2,1,0:T(8,128)(2,1)}, u32[]{:S(2)}) copy-start(bf16[1,1024,2048]{2,1,0:T(8,128)(2,1)} %all-gather.5.cloned.1.call-done) | copy-start | bytes 12582916
  224.4 10.9 %copy-start.7 = (bf16[2048,4]{0,1:T(4,128)(2,1)S(1)}, bf16[2048,4]{0,1:T(4,128)(2,1)}, u32[]{:S(2)}) copy-start(bf16[2048,4]{0,1:T(4,128)(2,1)} %param.22) | copy-start | bytes 49156
  224.4 11.2 %copy-start.6 = (bf16[2048,64]{0,1:T(8,128)(2,1)S(1)}, bf16[2048,64]{0,1:T(8,128)(2,1)}, u32[]{:S(2)}) copy-start(bf16[2048,64]{0,1:T(8,128)(2,1)} %param.23) | copy-start | bytes 786436
  224.4 62.0 %all-to-all-start.2 = ((bf16[6,64,2048]{2,0,1:T(8,128)(2,1)}), bf16[6,64,2048]{2,0,1:T(8,128)(2,1)}, u32[]{:S(2)}, u32[]{:S(2)}) async-start(bf16[6,64,2048]{2,0,1:T(8,128)(2,1)} %copy.51), calls=%async_computation.3 | async-start | bytes 4194304 | tf_op jit(solution)/shard_map/all_to_all | solution.py:137
Sparse Core Ops, SparseCore 0:
  93.5 64.3 all-gather.2
  159.7 56.0 all-gather.4
  219.0 31.9 reduce-scatter.1
where the time goes:
time: 303 us
  waiting for transfers between devices  151 us (50%)
  blocking collectives  63.1 us (21%)
  local copies, waits for them, and re-layouts  27.7 us (9%)
  matrix products  18 us (6%)
  starting transfers between devices  16.7 us (6%)
  between operations  14.2 us (5%)
  other arithmetic  12.1 us (4%)
    all_to_all x1, blocking collectives, expert_half(): lax.all_to_all(sending, 'ep', split_axis=1, concat_axis=1, tiled=True)  63.1 us
    all_gather x1, waiting for transfers between devices, expert_half(): received = lax.all_gather(arrived, 'tp', axis=0, tiled=True)  58.8 us
    all_to_all x1, waiting for transfers between devices, expert_half(): lax.all_to_all(summed, 'ep', split_axis=1, concat_axis=1, tiled=True)  49.9 us
    all_gather x1, waiting for transfers between devices, expert_half(): down_whole = lax.all_gather(down_weight, 'tp', axis=1, tiled=True)  26.5 us
    all_to_all x1, waiting for transfers between devices, expert_half(): lax.all_to_all(hidden, 'tp', split_axis=0, concat_axis=3, tiled=True)  14.8 us
    all_to_all x1, starting transfers between devices, expert_half(): lax.all_to_all(summed, 'ep', split_axis=1, concat_axis=1, tiled=True)  10.9 us
    scatter x1, local copies, waits for them, and re-layouts, dispatch_rows(): table.at[slot_index.reshape(-1), flat.reshape(-1)]  9.28 us
  transfers between devices with their start and end apart: 6, of which 4 were waited for; matrix products, arithmetic and copies ran while one was open for 11% of the time, Pallas kernels for 0%

commit v1 on v0

--- a/solution.py
+++ b/solution.py
@@ -116,7 +116,10 @@
     received = lax.all_gather(arrived, "tp", axis=0, tiled=True)
     held = gate_weight.shape[0]
     model = received.shape[2]
-    down_whole = lax.all_gather(down_weight, "tp", axis=1, tiled=True)
+    count_2 = lax.axis_size("tp")
+    parts = jnp.stack([down_weight for _ in range(count_2)])
+    parts = lax.all_to_all(parts, "tp", split_axis=0, concat_axis=0)
+    down_whole = jnp.concatenate(parts, axis=1)
     all_slots = received.reshape(received.shape[0], -1, held, model)
     gate = jnp.einsum("csed,edh->cseh", all_slots, gate_weight, preferred_element_type=jnp.float32)
     upward = jnp.einsum("csed,edh->cseh", all_slots, up_weight, preferred_element_type=jnp.float32)

time: 303 us -> 343 us (1.13)
  waiting for transfers between devices: 151 us -> 168 us
  blocking collectives: 63.1 us -> 78.8 us
    all_to_all x1, waiting for transfers between devices: 14.8 us -> 50.6 us  [expert_half(): parts = lax.all_to_all(parts, 'tp', split_axis=0, concat_axis=0)]
    all_gather x1 -> x0, waiting for transfers between devices: 26.5 us -> none  [expert_half(): down_whole = lax.all_gather(down_weight, 'tp', axis=1, tiled=True)]
    all_to_all x0 -> x1, blocking collectives: none -> 15.7 us  [expert_half(): lax.all_to_all(hidden, 'tp', split_axis=0, concat_axis=3, tiled=True)]
    all_gather x1, waiting for transfers between devices: 58.8 us -> 64.5 us  [expert_half(): received = lax.all_gather(arrived, 'tp', axis=0, tiled=True)]
  transfers between devices with their start and end apart: 6 -> 5, of which waited for: 4 -> 4; matrix products, arithmetic and copies ran while one was open for 11% -> 9% of each run, Pallas kernels for 0% -> 0%
where the time goes in v1:
time: 343 us; the launch traced here: 342 us
  waiting for transfers between devices  168 us (49%)
  blocking collectives  78.8 us (23%)
  local copies, waits for them, and re-layouts  28.5 us (8%)
  matrix products  20.3 us (6%)
  starting transfers between devices  18 us (5%)
  between operations  14.5 us (4%)
  other arithmetic  13.8 us (4%)
    all_gather x1, waiting for transfers between devices, expert_half(): received = lax.all_gather(arrived, 'tp', axis=0, tiled=True)  64.5 us
    all_to_all x1, blocking collectives, expert_half(): lax.all_to_all(sending, 'ep', split_axis=1, concat_axis=1, tiled=True)  63.1 us
    all_to_all x1, waiting for transfers between devices, expert_half(): parts = lax.all_to_all(parts, 'tp', split_axis=0, concat_axis=0)  50.6 us
    all_to_all x1, waiting for transfers between devices, expert_half(): lax.all_to_all(summed, 'ep', split_axis=1, concat_axis=1, tiled=True)  49.9 us
    all_to_all x1, blocking collectives, expert_half(): lax.all_to_all(hidden, 'tp', split_axis=0, concat_axis=3, tiled=True)  15.7 us
    all_to_all x1, starting transfers between devices, expert_half(): lax.all_to_all(summed, 'ep', split_axis=1, concat_axis=1, tiled=True)  10.9 us
    scatter x1, local copies, waits for them, and re-layouts, dispatch_rows(): table.at[slot_index.reshape(-1), flat.reshape(-1)]  9.28 us
    dot_general x4, matrix products, expert_half(): jnp.einsum('cseh,ehd->csed', swapped[:, :, :, part * hid_part:(part + 1)...  7.2 us
  transfers between devices with their start and end apart: 5, of which 4 were waited for; matrix products, arithmetic and copies ran while one was open for 9% of the time, Pallas kernels for 0%

profile of v1, /device:TPU:8, one launch (start us, length us, event | category | flops | bytes accessed | tf_op | source)
XLA Modules:
  0.0 342.1 jit_solution(14248207960212915643)
XLA Ops:
  9.5 1.8 multiply_reduce_fusion
  11.3 2.0 convert_element_type.227
  13.9 9.3 %scatter_fusion = s32[6,64]{1,0:T(8,128)S(1)} fusion(s32[6,64]{1,0:T(8,128)S(1)} %broadcast_in_dim.11, s32[192]{0:T(256)S(1)} %bitcast.131, s32[192]{0:T(256)S(1)} %and_select_fusion.1), kind=kCustom, calls=%fused_computation.2 | custom fusion | bytes 3840 | tf_op jit(solution)/shard_map/scatter | solution.py:91
  23.5 1.3 fusion.26
  24.8 2.5 gather_fusion
  27.2 1.0 copy_select_fusion
  28.2 63.1 %all_to_all.33 = bf16[6,64,2048]{2,0,1:T(8,128)(2,1)S(1)} all-to-all(bf16[6,64,2048]{2,0,1:T(8,128)(2,1)S(1)} %copy_select_fusion), channel_id=1, replica_groups=mesh['ep'=64,'tp'=4] {'ep'}, dimensions={1} | all-to-all | bytes 3145728 | tf_op jit(solution)/shard_map/all_to_all | solution.py:115
  91.4 2.0 copy.48
  93.4 64.5 %all-gather.2.cloned.1.call-done = bf16[24,64,2048]{2,1,0:T(8,128)(2,1)} async-done(((bf16[6,64,2048]{2,1,0:T(8,128)(2,1)}), bf16[24,64,2048]{2,1,0:T(8,128)(2,1)}) %all-gather.2.cloned.1.call-update) | async-done | bytes 6291472 | tf_op jit(solution)/shard_map/all_gather | solution.py:116
  157.9 4.8 %fusion.23 = f32[24,64,256]{2,1,0:T(8,128)S(1)} fusion(bf16[24,64,2048]{2,1,0:T(8,128)(2,1)} %all-gather.2.cloned.1.call-done, bf16[1,2048,256]{2,1,0:T(8,128)(2,1)S(1)} %copy-done.9), kind=kOutput, calls=%fused_computation.46 | convolution fusion | flops 1610612736 | bytes 8912896 | tf_op jit(solution)/shard_map/csed,edh->cseh/dot_general | solution.py:124
  162.8 2.1 fusion.16
  164.9 15.7 %all_to_all.34 = bf16[24,64,1,256]{3,1,2,0:T(8,128)(2,1)S(1)} all-to-all(bf16[24,64,1,256]{3,1,2,0:T(8,128)(2,1)S(1)} %fusion.16), channel_id=1, replica_groups=mesh['ep'=64,'tp'=4] {'tp'}, dimensions={0} | all-to-all | bytes 1572864 | tf_op jit(solution)/shard_map/all_to_all | solution.py:127
  180.6 2.5 stack.2
  183.1 5.0 %all-to-all-start.2 = ((bf16[4,1,256,2048]{3,2,1,0:T(8,128)(2,1)}), bf16[4,1,256,2048]{3,2,1,0:T(8,128)(2,1)}, u32[]{:S(2)}, u32[]{:S(2)}) async-start(bf16[4,1,256,2048]{3,2,1,0:T(8,128)(2,1)} %stack.2), calls=%async_computation.3 | async-start | bytes 8388608 | tf_op jit(solution)/shard_map/all_to_all | solution.py:121
  188.3 2.2 fusion
  190.6 2.0 fusion.17
  192.7 1.9 collective-permute-start
  194.7 2.9 collective-permute-done
  197.7 3.2 convolution_convert_fusion
  202.2 50.6 %all-to-all-done.2 = bf16[4,1,256,2048]{3,2,1,0:T(8,128)(2,1)} async-done(((bf16[4,1,256,2048]{3,2,1,0:T(8,128)(2,1)}), bf16[4,1,256,2048]{3,2,1,0:T(8,128)(2,1)}, u32[]{:S(2)}, u32[]{:S(2)}) %all-to-all-start.2) | async-done | bytes 4194336 | tf_op jit(solution)/shard_map/all_to_all | solution.py:121
  252.8 1.8 fusion.3
  254.6 1.8 fusion.4
  256.4 1.8 fusion.5
  258.2 1.8 fusion.6
  260.0 1.4 fusion.11
  261.4 2.2 copy.51
  263.6 10.9 %all-to-all-start.3 = ((bf16[6,64,2048]{2,0,1:T(8,128)(2,1)}), bf16[6,64,2048]{2,0,1:T(8,128)(2,1)}, u32[]{:S(2)}, u32[]{:S(2)}) async-start(bf16[6,64,2048]{2,0,1:T(8,128)(2,1)} %copy.51), calls=%async_computation.4 | async-start | bytes 4194304 | tf_op jit(solution)/shard_map/all_to_all | solution.py:140
  275.6 49.9 %all-to-all-done.3 = bf16[6,64,2048]{2,0,1:T(8,128)(2,1)} async-done(((bf16[6,64,2048]{2,0,1:T(8,128)(2,1)}), bf16[6,64,2048]{2,0,1:T(8,128)(2,1)}, u32[]{:S(2)}, u32[]{:S(2)}) %all-to-all-start.3) | async-done | bytes 1572896 | tf_op jit(solution)/shard_map/all_to_all | solution.py:140
  325.6 2.5 copy.52
  328.0 2.0 gather_fusion.1
  330.1 2.1 reshape.563
  332.2 3.1 multiply_reduce_fusion.1
  (75 shorter events, 5.8 us)
Async XLA Ops:
  7.2 190.5 %copy-start = (bf16[256,2048]{1,0:T(8,128)(2,1)S(1)}, bf16[256,2048]{1,0:T(8,128)(2,1)}, u32[]{:S(2)}) copy-start(bf16[256,2048]{1,0:T(8,128)(2,1)} %param.19) | copy-start | bytes 3145732
  7.2 4.2 %copy-start.1 = (bf16[384,2048]{1,0:T(8,128)(2,1)S(1)}, bf16[384,2048]{1,0:T(8,128)(2,1)}, u32[]{:S(2)}) copy-start(bf16[384,2048]{1,0:T(8,128)(2,1)} %param.20) | copy-start | bytes 4718596
  7.2 150.7 %all-gather.2.cloned.1.call-start = ((), (), s32[]{:S(2)}) async-start(), calls=%async_computation.6 | async-start | bytes 7864320 | tf_op jit(solution)/shard_map/all_gather | solution.py:116
  13.4 10.0 %copy-start.6 = (bf16[2048]{0:T(1024)(128)(2,1)S(1)}, bf16[2048]{0:T(1024)(128)(2,1)}, u32[]{:S(2)}) copy-start(bf16[2048]{0:T(1024)(128)(2,1)} %param.21) | copy-start | bytes 12292
  91.4 66.6 %copy-start.9 = (bf16[1,2048,256]{2,1,0:T(8,128)(2,1)S(1)}, bf16[1,2048,256]{2,1,0:T(8,128)(2,1)}, u32[]{:S(2)}) copy-start(bf16[1,2048,256]{2,1,0:T(8,128)(2,1)} %param.25) | copy-start | bytes 3145732
  157.9 4.8 %copy-start.8 = (bf16[24,64,2048]{2,1,0:T(8,128)(2,1)S(1)}, bf16[24,64,2048]{2,1,0:T(8,128)(2,1)}, u32[]{:S(2)}) copy-start(bf16[24,64,2048]{2,1,0:T(8,128)(2,1)} %all-gather.2.cloned.1.call-done) | copy-start | bytes 18874372
  157.9 4.9 %copy-start.10 = (bf16[1,2048,256]{2,1,0:T(8,128)(2,1)S(1)}, bf16[1,2048,256]{2,1,0:T(8,128)(2,1)}, u32[]{:S(2)}) copy-start(bf16[1,2048,256]{2,1,0:T(8,128)(2,1)} %param.26) | copy-start | bytes 3145732
  164.9 15.7 %copy-start.3 = (bf16[1,256,2048]{2,1,0:T(8,128)(2,1)S(1)}, bf16[1,256,2048]{2,1,0:T(8,128)(2,1)}, u32[]{:S(2)}) copy-start(bf16[1,256,2048]{2,1,0:T(8,128)(2,1)} %param.27) | copy-start | bytes 3145732
  183.1 5.2 %copy-start.7 = (bf16[2048]{0:T(1024)(128)(2,1)S(1)}, bf16[2048]{0:T(1024)(128)(2,1)}, u32[]{:S(2)}) copy-start(bf16[2048]{0:T(1024)(128)(2,1)} %param.15) | copy-start | bytes 12292
  183.1 69.7 %all-to-all-start.2 = ((bf16[4,1,256,2048]{3,2,1,0:T(8,128)(2,1)}), bf16[4,1,256,2048]{3,2,1,0:T(8,128)(2,1)}, u32[]{:S(2)}, u32[]{:S(2)}) async-start(bf16[4,1,256,2048]{3,2,1,0:T(8,128)(2,1)} %stack.2), calls=%async_computation.3 | async-start | bytes 8388608 | tf_op jit(solution)/shard_map/all_to_all | solution.py:121
  188.1 147.2 %reduce-scatter.2.cloned.1.call-start = ((), (), s32[]{:S(2)}) async-start(), calls=%async_computation.5 | async-start | bytes 2621440 | tf_op jit(solution)/shard_map/reduce_scatter | solution.py:67
  188.3 2.3 copy-start.2
  190.6 4.1 %copy-start.12 = (bf16[256]{0:T(256)(128)(2,1)S(1)}, bf16[256]{0:T(256)(128)(2,1)}, u32[]{:S(2)}) copy-start(bf16[256]{0:T(256)(128)(2,1)} %param.18) | copy-start | bytes 1540
  190.6 7.1 %copy-start.11 = (bf16[1,256,256]{2,1,0:T(8,128)(2,1)S(1)}, bf16[1,256,256]{2,1,0:T(8,128)(2,1)}, u32[]{:S(2)}) copy-start(bf16[1,256,256]{2,1,0:T(8,128)(2,1)} %param.17) | copy-start | bytes 393220
  192.7 5.0 %collective-permute-start = (bf16[15,256]{1,0:T(8,128)(2,1)S(1)}, bf16[15,256]{1,0:T(8,128)(2,1)S(1)}, u32[]{:S(2)}, u32[]{:S(2)}) collective-permute-start(bf16[15,256]{1,0:T(8,128)(2,1)S(1)} %slice.135), channel_id=1, source_target_pairs={{0,4},{4,8},{8,12},{12,16},{16,20},{20,24},{24,28},{28,32},{32,36}... | collective-permute-start | bytes 23048 | tf_op jit(solution)/shard_map/ppermute | solution.py:13
  263.6 10.9 %copy-start.5 = (bf16[2048,4]{0,1:T(4,128)(2,1)S(1)}, bf16[2048,4]{0,1:T(4,128)(2,1)}, u32[]{:S(2)}) copy-start(bf16[2048,4]{0,1:T(4,128)(2,1)} %param.22) | copy-start | bytes 49156
  263.6 11.1 %copy-start.4 = (bf16[2048,64]{0,1:T(8,128)(2,1)S(1)}, bf16[2048,64]{0,1:T(8,128)(2,1)}, u32[]{:S(2)}) copy-start(bf16[2048,64]{0,1:T(8,128)(2,1)} %param.23) | copy-start | bytes 786436
  263.6 62.0 %all-to-all-start.3 = ((bf16[6,64,2048]{2,0,1:T(8,128)(2,1)}), bf16[6,64,2048]{2,0,1:T(8,128)(2,1)}, u32[]{:S(2)}, u32[]{:S(2)}) async-start(bf16[6,64,2048]{2,0,1:T(8,128)(2,1)} %copy.51), calls=%async_computation.4 | async-start | bytes 4194304 | tf_op jit(solution)/shard_map/all_to_all | solution.py:140
Sparse Core Ops, SparseCore 0:
  93.5 64.3 all-gather.1
  201.1 51.0 reduce-scatter.1
